TPU v7x, 32 devices: a whole 2x2x4 slice. The times are simulated.
32 devices in a mesh: sp: 16 (over z, y, x), tp: 2 (over core).
Axes of the slice: x: 2, y: 2, z: 4, core: 2. Of those that a mesh axis runs over, the one named last changes fastest.
Arguments:
- queries: bfloat16 [8192, 2048], P('sp', 'tp'), may hold values from -6 to 6
- key_rows: bfloat16 [8192, 512], P('sp', 'tp'), may hold values from -6 to 6
- values: bfloat16 [8192, 512], P('sp', 'tp'), may hold values from -6 to 6
- sink_logit: float32 [32], P('tp'), may hold values from 4 to 10
- residual_in: bfloat16 [8192, 2048], P(('sp', 'tp')), may hold values from -6 to 6
- out_weight: bfloat16 [2048, 2048], P('tp'), may hold values from -0.125 to 0.125
- norm_gain: float32 [2048], replicated, may hold values from 0.1 to 1.9
- gate_weight: bfloat16 [2048, 5632], P('sp', 'tp'), may hold values from -0.125 to 0.125
- up_weight: bfloat16 [2048, 5632], P('sp', 'tp'), may hold values from -0.125 to 0.125
- down_weight: bfloat16 [5632, 2048], P('tp', 'sp'), may hold values from -0.078125 to 0.078125
Outputs:
- layer_out: bfloat16 [8192, 2048], P(('sp', 'tp'))
All inputs are finite; a program needn't handle non-finite values.
Results may differ from a plain program's by a relative error of at most 0.013.
Values may be sent and summed in bfloat16 or wider, within the bound.
A program may use at most 128 MiB of HBM per device.

v0:
```python
import jax
import jax.numpy as jnp
from jax import lax
from jax.sharding import PartitionSpec as P

HEAD_DIM = 64
WINDOW = 128


def with_halo(block, sides, width):
    for axis, dim in sides:
        count = lax.axis_size(axis)
        forward = [(i, i + 1) for i in range(count - 1)]
        backward = [(target, source) for source, target in forward]
        low = lax.ppermute(
            lax.slice_in_dim(block, block.shape[dim] - width, None, axis=dim), axis, forward
        )
        high = lax.ppermute(lax.slice_in_dim(block, 0, width, axis=dim), axis, backward)
        block = jnp.concatenate([low, block, high], axis=dim)
    return block


def rms_scale(mixed_rows, norm_gain):
    inverse = lax.rsqrt(jnp.mean(mixed_rows * mixed_rows, axis=-1, keepdims=True) + 1e-06)
    return (mixed_rows * inverse * norm_gain).astype(jnp.bfloat16)


def attend_window(queries, padded, offset, total_rows, sink_logit):
    rows_here = queries.shape[0]
    block_count = rows_here // WINDOW
    heads_here = queries.shape[1] // HEAD_DIM
    kv_here = padded.shape[1] // (2 * HEAD_DIM)
    group_size = heads_here // kv_here
    blocks = padded.reshape(block_count + 2, WINDOW, padded.shape[1])
    banded = jnp.concatenate([blocks[:-2], blocks[1:-1], blocks[2:]], axis=1)
    key_band = banded[:, :, : kv_here * HEAD_DIM].reshape(
        block_count, 3 * WINDOW, kv_here, HEAD_DIM
    )
    value_band = banded[:, :, kv_here * HEAD_DIM :].reshape(
        block_count, 3 * WINDOW, kv_here, HEAD_DIM
    )
    grouped = queries.reshape(block_count, WINDOW, kv_here, group_size, HEAD_DIM)
    scores = jnp.einsum(
        "nqkgd,nskd->nkgqs", grouped, key_band, preferred_element_type=jnp.float32
    ) * HEAD_DIM ** (-0.5)
    block_start = offset + jnp.arange(block_count, dtype=jnp.int32)[:, None] * WINDOW
    query_pos = block_start + jnp.arange(WINDOW, dtype=jnp.int32)[None, :]
    key_pos = block_start - WINDOW + jnp.arange(3 * WINDOW, dtype=jnp.int32)[None, :]
    valid = jnp.abs(query_pos[:, :, None] - key_pos[:, None, :]) <= WINDOW
    valid = valid & ((key_pos >= 0) & (key_pos < total_rows))[:, None, :]
    scores = jnp.where(valid[:, None, None], scores, -1e30)
    sink_grid = sink_logit.reshape(kv_here, group_size)[None, :, :, None, None]
    peak = jnp.maximum(jnp.max(scores, axis=-1, keepdims=True), sink_grid)
    weights_raw = jnp.exp(scores - peak)
    denom = jnp.sum(weights_raw, axis=-1, keepdims=True) + jnp.exp(sink_grid - peak)
    probs = (weights_raw / denom).astype(jnp.bfloat16)
    output = jnp.einsum("nkgqs,nskd->nqkgd", probs, value_band, preferred_element_type=jnp.float32)
    return output.astype(jnp.bfloat16).reshape(rows_here, heads_here * HEAD_DIM)


def shards(
    queries,
    key_rows,
    values,
    sink_logit,
    residual_in,
    out_weight,
    norm_gain,
    gate_weight,
    up_weight,
    down_weight,
):
    rows_here = queries.shape[0]
    row_share = rows_here // lax.axis_size("tp")
    joined = jnp.concatenate([key_rows, values], axis=1)
    padded = with_halo(joined, (("sp", 0),), WINDOW)
    offset = lax.axis_index("sp") * rows_here
    attended = attend_window(queries, padded, offset, rows_here * lax.axis_size("sp"), sink_logit)
    partial_value = jnp.dot(attended, out_weight, preferred_element_type=jnp.float32)
    summed = lax.psum(partial_value.astype(jnp.bfloat16), "tp").astype(jnp.float32)
    whole_residual = lax.all_gather(residual_in, "tp", axis=0, tiled=True)
    mixed_whole = whole_residual.astype(jnp.float32) + summed
    normed = rms_scale(mixed_whole, norm_gain)
    mixed_rows = lax.dynamic_slice_in_dim(
        mixed_whole, lax.axis_index("tp") * row_share, row_share, 0
    )
    gate_full, up_full = (
        lax.all_gather(gate_weight, "sp", axis=0, tiled=True),
        lax.all_gather(up_weight, "sp", axis=0, tiled=True),
    )
    down_full = lax.all_gather(down_weight, "sp", axis=1, tiled=True)
    gate_pre = jnp.dot(normed, gate_full, preferred_element_type=jnp.float32)
    up_pre = jnp.dot(normed, up_full, preferred_element_type=jnp.float32)
    hidden = (jax.nn.silu(gate_pre) * up_pre).astype(jnp.bfloat16)
    result = mixed_rows + lax.psum_scatter(
        jnp.dot(hidden, down_full, preferred_element_type=jnp.float32).astype(jnp.bfloat16),
        "tp",
        scatter_dimension=0,
        tiled=True,
    ).astype(jnp.float32)
    return result.astype(jnp.bfloat16)


def solution(mesh):
    return jax.shard_map(
        shards,
        mesh=mesh,
        in_specs=(
            P("sp", "tp"),
            P("sp", "tp"),
            P("sp", "tp"),
            P("tp"),
            P(("sp", "tp"), None),
            P("tp", None),
            P(),
            P("sp", "tp"),
            P("sp", "tp"),
            P("tp", "sp"),
        ),
        out_specs=P(("sp", "tp"), None),
        check_vma=False,
    )
```

profile of v0, /device:TPU:0, one launch (start us, length us, event | category | flops | bytes accessed | tf_op | source)
XLA Modules:
  0.0 577.9 jit_solution(7565747926765776180)
XLA Ops:
  6.5 0.0 copy-start.1
  6.5 0.0 all-gather.5.cloned.1.call-start
  6.5 1.0 constant_dynamic-update-slice_fusion.1
  7.5 1.0 constant_dynamic-update-slice_fusion
  8.5 4.9 collective-permute-start
  13.4 1.3 collective-permute-start.1
  14.7 0.0 all-gather.5.cloned.1.call-update
  14.7 0.0 all-reduce.2.cloned.1.call-start
  14.8 0.1 iota_add_fusion
  14.9 0.1 compare_and_fusion
  14.9 1.0 copy.17
  15.9 0.1 iota_add_fusion.1
  16.0 4.1 reshape.117
  20.2 0.0 copy-done.1
  20.2 0.1 max.18
  20.3 0.6 fusion.9
  20.8 0.0 collective-permute-done
  20.8 0.1 collective-permute-done.1
  21.0 1.8 pad_maximum_fusion.2
  22.8 1.4 copy.16
  24.1 1.0 copy.18
  25.1 1.5 pad_maximum_fusion
  26.6 0.2 fusion.14
  26.8 2.5 fusion.1
  29.3 0.1 broadcast_maximum_fusion
  29.4 3.4 fusion
  32.7 0.1 exponential_add_fusion
  32.8 0.0 copy-start.2
  32.9 3.8 fusion.6
  36.6 0.9 copy.22
  37.5 0.0 copy-done.2
  37.5 3.8 convolution_convert_fusion
  41.4 0.0 all-reduce.2.cloned.1.call-update
  41.4 0.0 all-gather.7.cloned.1.call-start
  41.4 0.7 all-gather.7.cloned.1.call-update
  42.1 0.0 all-gather.11.cloned.1.call-start
  42.2 0.5 all-gather.11.cloned.1.call-update
  42.7 0.0 all-gather.9.cloned.1.call-start
  42.8 0.5 all-gather.9.cloned.1.call-update
  43.3 0.0 copy-start.3
  43.3 0.0 reduce-scatter.2.cloned.1.call-start
  43.4 0.0 all-gather.5.cloned.1.call-done
  43.4 0.0 copy-start
  43.4 22.3 %all-reduce.2.cloned.1.call-done = bf16[512,2048]{1,0:T(8,128)(2,1)} async-done(((bf16[512,2048]{1,0:T(8,128)(2,1)}), bf16[512,2048]{1,0:T(8,128)(2,1)}) %all-reduce.2.cloned.1.call-update) | async-done | bytes 2097168 | tf_op jit(solution)/shard_map/psum | solution.py:80
  65.7 4.9 convert_add_fusion
  70.6 140.5 %all-gather.7.cloned.1.call-done = bf16[2048,2816]{1,0:T(8,128)(2,1)} async-done(((bf16[128,2816]{1,0:T(8,128)(2,1)}), bf16[2048,2816]{1,0:T(8,128)(2,1)}) %all-gather.7.cloned.1.call-update) | async-done | bytes 11534352 | tf_op jit(solution)/shard_map/all_gather | solution.py:88
  211.1 0.0 copy-done.3
  211.1 0.0 copy-done
  211.1 12.8 %fusion.13 = f32[512,2816]{1,0:T(8,128)} fusion(bf16[2048,2816]{1,0:T(8,128)(2,1)} %all-gather.7.cloned.1.call-done, f32[2048]{0:T(1024)S(1)} %copy-done.3, f32[512]{0:T(512)S(1)} %add_rsqrt_fusion, bf16[512,2048]{1,0:T(8,128)(2,1)} %all-reduce.2.cloned.1.call-done, bf16[512,2048]{1,0:T(8,128)(2,1)S(1)} %copy-done), kind=kOutput, calls=%fused_computation.37 | convolution fusion | flops 5911871488 | bytes 21506048 | tf_op jit(solution)/shard_map/dot_general | solution.py:92
  223.9 170.0 %all-gather.11.cloned.1.call-done = bf16[2816,2048]{1,0:T(8,128)(2,1)} async-done(((bf16[2816,128]{1,0:T(8,128)(2,1)}), bf16[2816,2048]{1,0:T(8,128)(2,1)}) %all-gather.11.cloned.1.call-update) | async-done | bytes 11534352 | tf_op jit(solution)/shard_map/all_gather | solution.py:91
  393.9 142.2 %all-gather.9.cloned.1.call-done = bf16[2048,2816]{1,0:T(8,128)(2,1)} async-done(((bf16[128,2816]{1,0:T(8,128)(2,1)}), bf16[2048,2816]{1,0:T(8,128)(2,1)}) %all-gather.9.cloned.1.call-update) | async-done | bytes 11534352 | tf_op jit(solution)/shard_map/all_gather | solution.py:89
  536.1 23.6 %convolution_convert_fusion.1 = bf16[512,2048]{1,0:T(8,128)(2,1)} fusion(bf16[2816,2048]{1,0:T(8,128)(2,1)} %all-gather.11.cloned.1.call-done, f32[512,2816]{1,0:T(8,128)} %fusion.13, bf16[2048,2816]{1,0:T(8,128)(2,1)} %all-gather.9.cloned.1.call-done, f32[2048]{0:T(1024)S(1)} %copy-done.3, f32[512]{0:T(512)S(1)} %add_rsqrt_fusion, ...), kind=kOutput, calls=%fused_computation.11 | convolution fusion | flops 11827150848 | bytes 35137536 | tf_op jit(solution)/shard_map/dot_general | solution.py:96
  559.7 0.0 reduce-scatter.2.cloned.1.call-update
  559.7 8.1 %reduce-scatter.2.cloned.1.call-done = bf16[256,2048]{1,0:T(8,128)(2,1)} async-done(((bf16[512,2048]{1,0:T(8,128)(2,1)}), bf16[256,2048]{1,0:T(8,128)(2,1)}) %reduce-scatter.2.cloned.1.call-update) | async-done | bytes 1048592 | tf_op jit(solution)/shard_map/reduce_scatter | solution.py:95
  567.8 3.2 add_convert_fusion
  (3 shorter events, 0.0 us)
Async XLA Ops:
  6.5 13.6 %copy-start.1 = (f32[16]{0:T(128)S(1)}, f32[16]{0:T(128)}, u32[]{:S(2)}) copy-start(f32[16]{0:T(128)} %param.13) | copy-start | bytes 196
  6.5 36.8 %all-gather.5.cloned.1.call-start = ((), (), s32[]{:S(2)}) async-start(), calls=%async_computation.1 | async-start | bytes 3145728 | tf_op jit(solution)/shard_map/all_gather | solution.py:81
  8.5 12.3 %collective-permute-start = (bf16[128,512]{1,0:T(8,128)(2,1)S(1)}, bf16[128,512]{1,0:T(8,128)(2,1)S(1)}, u32[]{:S(2)}, u32[]{:S(2)}) collective-permute-start(bf16[128,512]{1,0:T(8,128)(2,1)S(1)} %get-tuple-element.11), channel_id=1, source_target_pairs={{0,2},{2,4},{4,6},{6,8},{8,10},{10,12},{12,14},{14,16},{16,18},{18... | collective-permute-start | bytes 393224 | tf_op jit(solution)/shard_map/ppermute | solution.py:15
  13.4 7.6 %collective-permute-start.1 = (bf16[128,512]{1,0:T(8,128)(2,1)S(1)}, bf16[128,512]{1,0:T(8,128)(2,1)}, u32[]{:S(2)}, u32[]{:S(2)}) collective-permute-start(bf16[128,512]{1,0:T(8,128)(2,1)S(1)} %get-tuple-element.12), channel_id=1, source_target_pairs={{2,0},{4,2},{6,4},{8,6},{10,8},{12,10},{14,12},{16,14},{18,16},{20... | collective-permute-start | bytes 393224 | tf_op jit(solution)/shard_map/ppermute | solution.py:18
  14.7 50.9 %all-reduce.2.cloned.1.call-start = ((), (), s32[]{:S(2)}) async-start(), calls=%async_computation.2 | async-start | bytes 4194304 | tf_op jit(solution)/shard_map/psum | solution.py:80
  32.8 4.7 copy-start.2
  41.4 169.7 %all-gather.7.cloned.1.call-start = ((), (), s32[]{:S(2)}) async-start(), calls=%async_computation.3 | async-start | bytes 12255232 | tf_op jit(solution)/shard_map/all_gather | solution.py:88
  42.1 351.7 %all-gather.11.cloned.1.call-start = ((), (), s32[]{:S(2)}) async-start(), calls=%async_computation.5 | async-start | bytes 12255232 | tf_op jit(solution)/shard_map/all_gather | solution.py:91
  42.7 493.4 %all-gather.9.cloned.1.call-start = ((), (), s32[]{:S(2)}) async-start(), calls=%async_computation.4 | async-start | bytes 12255232 | tf_op jit(solution)/shard_map/all_gather | solution.py:89
  43.3 167.8 %copy-start.3 = (f32[2048]{0:T(1024)S(1)}, f32[2048]{0:T(1024)}, u32[]{:S(2)}) copy-start(f32[2048]{0:T(1024)} %param.16) | copy-start | bytes 24580
  43.3 524.5 %reduce-scatter.2.cloned.1.call-start = ((), (), s32[]{:S(2)}) async-start(), calls=%async_computation.6 | async-start | bytes 3145728 | tf_op jit(solution)/shard_map/reduce_scatter | solution.py:95
  43.4 167.7 %copy-start = (bf16[512,2048]{1,0:T(8,128)(2,1)S(1)}, bf16[512,2048]{1,0:T(8,128)(2,1)}, u32[]{:S(2)}) copy-start(bf16[512,2048]{1,0:T(8,128)(2,1)} %all-gather.5.cloned.1.call-done) | copy-start | bytes 6291460
Sparse Core Ops, SparseCore 0:
  14.9 13.6 all-gather.4
  41.5 24.0 all-reduce.1
  68.4 142.5 all-gather.6
  213.6 180.2 all-gather.10
  396.5 139.5 all-gather.8
  559.9 7.9 reduce-scatter.1
where the time goes:
time: 578 us
  waiting for transfers between devices  485 us (84%)
  matrix products  46.6 us (8%)
  other arithmetic  15.7 us (3%)
  between operations  13.6 us (2%)
  local copies, waits for them, and re-layouts  10.6 us (2%)
  starting transfers between devices  6.37 us (1%)
    all_gather x1, waiting for transfers between devices, shards(): down_full = lax.all_gather(down_weight, 'sp', axis=1, tiled=True)  170 us
    all_gather x1, waiting for transfers between devices, shards(): lax.all_gather(up_weight, 'sp', axis=0, tiled=True)  142 us
    all_gather x1, waiting for transfers between devices, shards(): lax.all_gather(gate_weight, 'sp', axis=0, tiled=True)  141 us
    dot_general x1, matrix products, shards(): jnp.dot(hidden, down_full, preferred_element_type=jnp.float32)  23.6 us
    psum x1, waiting for transfers between devices, shards(): lax.psum(partial_value.astype(jnp.bfloat16), 'tp').astype(jnp.float32)  22.3 us
    dot_general x1, matrix products, shards(): gate_pre = jnp.dot(normed, gate_full, preferred_element_type=jnp.float32)  12.8 us
  transfers between devices with their start and end apart: 8, of which 6 were waited for; matrix products, arithmetic and copies ran while one was open for 8% of the time, Pallas kernels for 0%

commit v1 on v0

--- a/solution.py
+++ b/solution.py
@@ -88,7 +88,11 @@
         lax.all_gather(gate_weight, "sp", axis=0, tiled=True),
         lax.all_gather(up_weight, "sp", axis=0, tiled=True),
     )
-    down_full = lax.all_gather(down_weight, "sp", axis=1, tiled=True)
+
+    def follow_waves(m, d_out):
+        return jnp.concatenate(lax.all_gather(m, "sp"), axis=d_out)
+
+    down_full = follow_waves(down_weight, 1)
     gate_pre = jnp.dot(normed, gate_full, preferred_element_type=jnp.float32)
     up_pre = jnp.dot(normed, up_full, preferred_element_type=jnp.float32)
     hidden = (jax.nn.silu(gate_pre) * up_pre).astype(jnp.bfloat16)

time: 578 us -> 542 us (0.938)
  waiting for transfers between devices: 485 us -> 429 us
  local copies, waits for them, and re-layouts: 10.6 us -> 26 us
    all_gather x1, waiting for transfers between devices: 170 us -> 141 us  [follow_waves(): return jnp.concatenate(lax.all_gather(m, 'sp'), axis=d_out)]
    reshape x0 -> x1, local copies, waits for them, and re-layouts: none -> 15.4 us  [follow_waves(): return jnp.concatenate(lax.all_gather(m, 'sp'), axis=d_out)]
    all_gather x1, waiting for transfers between devices: 141 us -> 127 us  [shards(): lax.all_gather(gate_weight, 'sp', axis=0, tiled=True)]
    all_gather x1, waiting for transfers between devices: 142 us -> 129 us  [shards(): lax.all_gather(up_weight, 'sp', axis=0, tiled=True)]
  transfers between devices with their start and end apart: 8 -> 8, of which waited for: 6 -> 6; matrix products, arithmetic and copies ran while one was open for 8% -> 11% of each run, Pallas kernels for 0% -> 0%
where the time goes in v1:
time: 542 us; the launch traced here: 541 us
  waiting for transfers between devices  429 us (79%)
  matrix products  50.4 us (9%)
  local copies, waits for them, and re-layouts  26 us (5%)
  other arithmetic  15.6 us (3%)
  between operations  13.6 us (3%)
  starting transfers between devices  6.37 us (1%)
    all_gather x1, waiting for transfers between devices, follow_waves(): return jnp.concatenate(lax.all_gather(m, 'sp'), axis=d_out)  141 us
    all_gather x1, waiting for transfers between devices, shards(): lax.all_gather(up_weight, 'sp', axis=0, tiled=True)  129 us
    all_gather x1, waiting for transfers between devices, shards(): lax.all_gather(gate_weight, 'sp', axis=0, tiled=True)  127 us
    dot_general x1, matrix products, shards(): jnp.dot(hidden, down_full, preferred_element_type=jnp.float32)  27.5 us
    psum x1, waiting for transfers between devices, shards(): lax.psum(partial_value.astype(jnp.bfloat16), 'tp').astype(jnp.float32)  22.3 us
    reshape x1, local copies, waits for them, and re-layouts, follow_waves(): return jnp.concatenate(lax.all_gather(m, 'sp'), axis=d_out)  15.4 us
    dot_general x1, matrix products, shards(): gate_pre = jnp.dot(normed, gate_full, preferred_element_type=jnp.float32)  12.8 us
  transfers between devices with their start and end apart: 8, of which 6 were waited for; matrix products, arithmetic and copies ran while one was open for 11% of the time, Pallas kernels for 0%

profile of v1, /device:TPU:0, one launch (start us, length us, event | category | flops | bytes accessed | tf_op | source)
XLA Modules:
  0.0 541.1 jit_solution(9308601286852341785)
XLA Ops:
  6.5 0.0 copy-start.1
  6.5 0.0 all-gather.6.cloned.1.call-start
  6.5 1.0 constant_dynamic-update-slice_fusion.1
  7.5 1.0 constant_dynamic-update-slice_fusion
  8.5 4.9 collective-permute-start
  13.4 1.3 collective-permute-start.1
  14.7 0.0 all-gather.6.cloned.1.call-update
  14.7 0.0 all-reduce.2.cloned.1.call-start
  14.8 0.1 iota_add_fusion
  14.9 0.1 compare_and_fusion
  14.9 1.0 copy.24
  15.9 0.1 iota_add_fusion.1
  16.0 4.1 reshape.126
  20.2 0.0 copy-done.1
  20.2 0.1 max.18
  20.3 0.6 fusion.9
  20.8 0.0 collective-permute-done
  20.8 0.1 collective-permute-done.1
  21.0 1.8 pad_maximum_fusion.2
  22.8 1.4 copy.23
  24.1 1.0 copy.25
  25.1 1.5 pad_maximum_fusion
  26.6 0.2 fusion.14
  26.8 2.5 fusion.1
  29.3 0.1 broadcast_maximum_fusion
  29.4 3.4 fusion
  32.7 0.1 exponential_add_fusion
  32.8 0.0 copy-start.2
  32.9 3.8 fusion.6
  36.6 0.9 copy.29
  37.5 0.0 copy-done.2
  37.5 3.8 convolution_convert_fusion
  41.4 0.0 all-reduce.2.cloned.1.call-update
  41.4 0.0 all-gather.12.cloned.1.call-start
  41.5 0.7 all-gather.12.cloned.1.call-update
  42.1 0.0 all-gather.8.cloned.1.call-start
  42.2 0.5 all-gather.8.cloned.1.call-update
  42.7 0.0 all-gather.10.cloned.1.call-start
  42.8 0.5 all-gather.10.cloned.1.call-update
  43.3 0.0 reduce-scatter.2.cloned.1.call-start
  43.4 0.0 all-gather.6.cloned.1.call-done
  43.4 22.3 %all-reduce.2.cloned.1.call-done = bf16[512,2048]{1,0:T(8,128)(2,1)} async-done(((bf16[512,2048]{1,0:T(8,128)(2,1)}), bf16[512,2048]{1,0:T(8,128)(2,1)}) %all-reduce.2.cloned.1.call-update) | async-done | bytes 2097168 | tf_op jit(solution)/shard_map/psum | solution.py:80
  65.7 4.8 convert_add_fusion
  70.5 140.6 %all-gather.12.cloned.1.call-done = bf16[45056,128]{1,0:T(8,128)(2,1)} async-done(((bf16[2816,128]{1,0:T(8,128)(2,1)}), bf16[45056,128]{1,0:T(8,128)(2,1)}) %all-gather.12.cloned.1.call-update) | async-done | bytes 11534352 | tf_op jit(solution)/shard_map/all_gather | solution.py:93
  211.1 0.0 copy-start
  211.1 0.0 copy-start.3
  211.1 15.4 %copy.30 = bf16[2816,16,128]{0,2,1:T(8,128)(2,1)} copy(bf16[2816,16,128]{2,0,1:T(8,128)(2,1)} %bitcast.45) | data formatting | bytes 23068672 | tf_op jit(solution)/shard_map/reshape | solution.py:93
  226.4 126.9 %all-gather.8.cloned.1.call-done = bf16[2048,2816]{1,0:T(8,128)(2,1)} async-done(((bf16[128,2816]{1,0:T(8,128)(2,1)}), bf16[2048,2816]{1,0:T(8,128)(2,1)}) %all-gather.8.cloned.1.call-update) | async-done | bytes 11534352 | tf_op jit(solution)/shard_map/all_gather | solution.py:88
  353.3 0.0 copy-done
  353.3 0.0 copy-done.3
  353.3 12.8 %fusion.13 = f32[512,2816]{1,0:T(8,128)} fusion(bf16[2048,2816]{1,0:T(8,128)(2,1)} %all-gather.8.cloned.1.call-done, f32[2048]{0:T(1024)S(1)} %copy-done.3, f32[512]{0:T(512)S(1)} %add_rsqrt_fusion, bf16[512,2048]{1,0:T(8,128)(2,1)} %all-reduce.2.cloned.1.call-done, bf16[512,2048]{1,0:T(8,128)(2,1)S(1)} %copy-done), kind=kOutput, calls=%fused_computation.37 | convolution fusion | flops 5911871488 | bytes 21506048 | tf_op jit(solution)/shard_map/dot_general | solution.py:96
  366.2 129.4 %all-gather.10.cloned.1.call-done = bf16[2048,2816]{1,0:T(8,128)(2,1)} async-done(((bf16[128,2816]{1,0:T(8,128)(2,1)}), bf16[2048,2816]{1,0:T(8,128)(2,1)}) %all-gather.10.cloned.1.call-update) | async-done | bytes 11534352 | tf_op jit(solution)/shard_map/all_gather | solution.py:89
  495.5 27.5 %convolution_convert_fusion.1 = bf16[512,2048]{1,0:T(8,128)(2,1)} fusion(bf16[2816,2048]{0,1:T(8,128)(2,1)} %bitcast.46, f32[512,2816]{1,0:T(8,128)} %fusion.13, bf16[2048,2816]{1,0:T(8,128)(2,1)} %all-gather.10.cloned.1.call-done, f32[2048]{0:T(1024)S(1)} %copy-done.3, f32[512]{0:T(512)S(1)} %add_rsqrt_fusion, ...), kind=kOutput, calls=%fused_computation.11 | convolution fusion | flops 11827150848 | bytes 35137536 | tf_op jit(solution)/shard_map/dot_general | solution.py:100
  523.0 0.0 reduce-scatter.2.cloned.1.call-update
  523.0 8.1 %reduce-scatter.2.cloned.1.call-done = bf16[256,2048]{1,0:T(8,128)(2,1)} async-done(((bf16[512,2048]{1,0:T(8,128)(2,1)}), bf16[256,2048]{1,0:T(8,128)(2,1)}) %reduce-scatter.2.cloned.1.call-update) | async-done | bytes 1048592 | tf_op jit(solution)/shard_map/reduce_scatter | solution.py:99
  531.1 3.2 add_convert_fusion
  (3 shorter events, 0.0 us)
Async XLA Ops:
  6.5 13.6 %copy-start.1 = (f32[16]{0:T(128)S(1)}, f32[16]{0:T(128)}, u32[]{:S(2)}) copy-start(f32[16]{0:T(128)} %param.13) | copy-start | bytes 196
  6.5 36.8 %all-gather.6.cloned.1.call-start = ((), (), s32[]{:S(2)}) async-start(), calls=%async_computation.1 | async-start | bytes 3145728 | tf_op jit(solution)/shard_map/all_gather | solution.py:81
  8.5 12.3 %collective-permute-start = (bf16[128,512]{1,0:T(8,128)(2,1)S(1)}, bf16[128,512]{1,0:T(8,128)(2,1)S(1)}, u32[]{:S(2)}, u32[]{:S(2)}) collective-permute-start(bf16[128,512]{1,0:T(8,128)(2,1)S(1)} %get-tuple-element.11), channel_id=1, source_target_pairs={{0,2},{2,4},{4,6},{6,8},{8,10},{10,12},{12,14},{14,16},{16,18},{18... | collective-permute-start | bytes 393224 | tf_op jit(solution)/shard_map/ppermute | solution.py:15
  13.4 7.6 %collective-permute-start.1 = (bf16[128,512]{1,0:T(8,128)(2,1)S(1)}, bf16[128,512]{1,0:T(8,128)(2,1)}, u32[]{:S(2)}, u32[]{:S(2)}) collective-permute-start(bf16[128,512]{1,0:T(8,128)(2,1)S(1)} %get-tuple-element.12), channel_id=1, source_target_pairs={{2,0},{4,2},{6,4},{8,6},{10,8},{12,10},{14,12},{16,14},{18,16},{20... | collective-permute-start | bytes 393224 | tf_op jit(solution)/shard_map/ppermute | solution.py:18
  14.7 50.9 %all-reduce.2.cloned.1.call-start = ((), (), s32[]{:S(2)}) async-start(), calls=%async_computation.2 | async-start | bytes 4194304 | tf_op jit(solution)/shard_map/psum | solution.py:80
  32.8 4.7 copy-start.2
  41.4 169.7 %all-gather.12.cloned.1.call-start = ((), (), s32[]{:S(2)}) async-start(), calls=%async_computation.6 | async-start | bytes 12255232 | tf_op jit(solution)/shard_map/all_gather | solution.py:93
  42.1 311.2 %all-gather.8.cloned.1.call-start = ((), (), s32[]{:S(2)}) async-start(), calls=%async_computation.3 | async-start | bytes 12255232 | tf_op jit(solution)/shard_map/all_gather | solution.py:88
  42.7 452.8 %all-gather.10.cloned.1.call-start = ((), (), s32[]{:S(2)}) async-start(), calls=%async_computation.4 | async-start | bytes 12255232 | tf_op jit(solution)/shard_map/all_gather | solution.py:89
  43.3 487.8 %reduce-scatter.2.cloned.1.call-start = ((), (), s32[]{:S(2)}) async-start(), calls=%async_computation.5 | async-start | bytes 3145728 | tf_op jit(solution)/shard_map/reduce_scatter | solution.py:99
  211.1 142.2 %copy-start = (bf16[512,2048]{1,0:T(8,128)(2,1)S(1)}, bf16[512,2048]{1,0:T(8,128)(2,1)}, u32[]{:S(2)}) copy-start(bf16[512,2048]{1,0:T(8,128)(2,1)} %all-gather.6.cloned.1.call-done) | copy-start | bytes 6291460
  211.1 142.2 %copy-start.3 = (f32[2048]{0:T(1024)S(1)}, f32[2048]{0:T(1024)}, u32[]{:S(2)}) copy-start(f32[2048]{0:T(1024)} %param.16) | copy-start | bytes 24580
Sparse Core Ops, SparseCore 0:
  14.9 13.6 all-gather.5
  41.5 24.0 all-reduce.1
  68.4 142.5 all-gather.11
  213.7 139.5 all-gather.7
  355.9 139.5 all-gather.9
  523.1 7.9 reduce-scatter.1
